TPU v7x, 32 devices: a whole 2x2x4 slice. The times are simulated.
32 devices in a mesh: dp: 4 (over y, x), kv: 4 (over z), tp: 2 (over core).
Axes of the slice: x: 2, y: 2, z: 4, core: 2. Of those that a mesh axis runs over, the one named last changes fastest.
Arguments:
- tokens: bfloat16 [256, 2048], P('dp', ('kv', 'tp')), parts along dimension 0, may hold values from -64 to 64, as said below
- lengths: int32 [32], P(('dp', 'kv', 'tp')), parts along dimension 0, may hold values from 1 to 8, 28 in all
- state: float32 [32, 16, 128, 128], P(('dp', 'kv', 'tp')), parts along dimension 0, may hold values from -1.8 to 1.8
- gain_first: float32 [2048], replicated, may hold values from 0.1 to 1.9
- first_gate: bfloat16 [2048, 5632], P(None, 'kv'), may hold values from -0.125 to 0.125
- first_up: bfloat16 [2048, 5632], P(None, 'kv'), may hold values from -0.125 to 0.125
- first_down: bfloat16 [5632, 2048], P('kv'), may hold values from -0.109375 to 0.109375
- gain_mix: float32 [2048], replicated, may hold values from 0.1 to 1.9
- query_weight: bfloat16 [2048, 2048], P(None, ('kv', 'tp')), may hold values from -0.125 to 0.125
- key_weight: bfloat16 [2048, 2048], P(None, ('kv', 'tp')), may hold values from -0.125 to 0.125
- value_weight: bfloat16 [2048, 2048], P(None, ('kv', 'tp')), may hold values from -0.125 to 0.125
- gating_weight: bfloat16 [2048, 2048], P(None, ('kv', 'tp')), may hold values from -0.125 to 0.125
- write_weight: bfloat16 [2048, 16], replicated, may hold values from -0.125 to 0.125
- forget_weight: bfloat16 [2048, 16], replicated, may hold values from -0.125 to 0.125
- forget_rate: float32 [16], replicated, may hold values from -4 to 1.5
- out_weight: bfloat16 [2048, 2048], P(None, ('kv', 'tp')), may hold values from -0.125 to 0.125
- gain_second: float32 [2048], replicated, may hold values from 0.1 to 1.9
- second_gate: bfloat16 [2048, 5632], P(None, 'kv'), may hold values from -0.125 to 0.125
- second_up: bfloat16 [2048, 5632], P(None, 'kv'), may hold values from -0.125 to 0.125
- second_down: bfloat16 [5632, 2048], P('kv'), may hold values from -0.109375 to 0.109375
Outputs:
- mixed_out: bfloat16 [256, 2048], P('dp', ('kv', 'tp')), parts along dimension 0
- new_state: float32 [32, 16, 128, 128], P(('dp', 'kv', 'tp')), parts along dimension 0
There are 4 independent parts, one for each index of `dp`. A program takes and returns all parts, laid end to end along the dimension named above; an argument that names none is the same for every part. Nothing has to cross between parts.
Inputs may be any that keep to these rules, and one draw needn't show every extreme that they name: Activations of the new tokens. `lengths`: the live new tokens of each sequence; within each independent group of 8 sequences (one part along dp) they sum to seven halves of 8, rounded down, and some sequence of each group has all 8 live.
All inputs are finite; a program needn't handle non-finite values.
Results may differ from a plain program's by a relative error of at most 0.0058.
Values may be sent and summed in bfloat16 or wider, within the bound.
A program may use at most 128 MiB of HBM per device.

v0:
```python
import math
import jax
import jax.numpy as jnp
from jax import lax
from jax.sharding import PartitionSpec as P

HEADS = 16
HEAD = 128
BLK = 8
EPSILON = 1e-06


def fold_step(gain, gate_cols, up_cols, portion):
    values = portion.astype(jnp.float32)
    scaled = (values * gain).astype(jnp.bfloat16)
    gate_acc = jnp.dot(scaled, gate_cols, preferred_element_type=jnp.float32)
    up_acc = jnp.dot(scaled, up_cols, preferred_element_type=jnp.float32)
    squares = jnp.sum(values * values, axis=1)
    return (gate_acc, up_acc, squares)


def finish_units(gate_acc, up_acc, squares, channels, down_rows):
    row_scale = lax.rsqrt(squares / channels + EPSILON)[:, None]
    hidden = (jax.nn.silu(gate_acc * row_scale) * (up_acc * row_scale)).astype(jnp.bfloat16)
    return jnp.dot(hidden, down_rows, preferred_element_type=jnp.float32)


def feed_forward(hidden_in, gain, w_gate, w_up, w_down):
    channels = gain.shape[0]
    paired = lax.all_to_all(hidden_in, "tp", split_axis=0, concat_axis=1, tiled=True)
    gate_acc, up_acc, squares = fold_step(
        gain, w_gate, w_up, lax.all_gather(paired, "kv", axis=1, tiled=True)
    )
    ffn_term = finish_units(gate_acc, up_acc, squares, channels, w_down)
    partial_value = lax.psum_scatter(ffn_term, "kv", scatter_dimension=1, tiled=True)
    summed = lax.all_to_all(partial_value, "tp", split_axis=1, concat_axis=0, tiled=True)
    return (hidden_in.astype(jnp.float32) + 0.5 * summed).astype(jnp.bfloat16)


def delta_block(query, key_in, value, gating, write_pre, forget_pre, rates, live, state):
    seq_count, block_len, head_count, head_size = query.shape
    precise = lax.Precision.HIGHEST
    query_unit = (
        query
        * lax.rsqrt(jnp.sum(query * query, axis=-1, keepdims=True) + EPSILON)
        / math.sqrt(head_size)
    )
    key_unit = key_in * lax.rsqrt(jnp.sum(key_in * key_in, axis=-1, keepdims=True) + EPSILON)
    live_rows = live[:, :, None]
    write_gate = jax.nn.sigmoid(write_pre) * live_rows
    forget = -jnp.exp(rates)[None, None, :] * jax.nn.softplus(forget_pre) * live_rows
    cumulative = jnp.cumsum(forget, axis=1)
    cum_heads = jnp.transpose(cumulative, (0, 2, 1))
    positions = jnp.arange(block_len)
    causal = positions[:, None] >= positions[None, :]
    strict = positions[:, None] > positions[None, :]
    differ = jnp.minimum(cum_heads[:, :, :, None] - cum_heads[:, :, None, :], 0.0)
    decay_mat = jnp.where(causal, jnp.exp(differ), 0.0)
    key_dots = jnp.einsum("sthd,suhd->shtu", key_unit, key_unit, precision=precise)
    write_heads = jnp.transpose(write_gate, (0, 2, 1))
    strict_part = jnp.where(strict, write_heads[:, :, :, None] * decay_mat * key_dots, 0.0)
    identity = jnp.eye(block_len, dtype=jnp.float32)
    squared = jnp.einsum("shtu,shuv->shtv", strict_part, strict_part, precision=precise)
    fourth = jnp.einsum("shtu,shuv->shtv", squared, squared, precision=precise)
    inverse = jnp.einsum(
        "shtu,shuv->shtv", identity - strict_part, identity + squared, precision=precise
    )
    inverse = jnp.einsum("shtu,shuv->shtv", inverse, identity + fourth, precision=precise)
    growth = jnp.exp(cumulative)
    target = jnp.einsum(
        "shtu,suhv->sthv", inverse, write_gate[..., None] * value, precision=precise
    )
    key_mix = jnp.einsum(
        "shtu,suhk->sthk", inverse, (write_gate * growth)[..., None] * key_unit, precision=precise
    )
    update = target - jnp.einsum("sthk,shkv->sthv", key_mix, state, precision=precise)
    scores = jnp.einsum("sthd,suhd->shtu", query_unit, key_unit, precision=precise) * decay_mat
    attend = jnp.einsum("sthk,shkv->sthv", query_unit * growth[..., None], state, precision=precise)
    attend = attend + jnp.einsum("shtu,suhv->sthv", scores, update, precision=precise)
    final_cum = cumulative[:, -1:, :]
    fading = jnp.exp(final_cum - cumulative)
    new_state = jnp.exp(final_cum[:, 0, :])[:, :, None, None] * state
    new_state = new_state + jnp.einsum(
        "sthk,sthv->shkv", key_unit * fading[..., None], update, precision=precise
    )
    normed = attend * lax.rsqrt(jnp.mean(attend * attend, axis=-1, keepdims=True) + EPSILON)
    normed = normed * jax.nn.silu(gating) * live[:, :, None, None]
    mixed_heads = normed.reshape(seq_count * block_len, head_count * head_size).astype(jnp.bfloat16)
    return (mixed_heads, new_state)


def per_device(
    tokens,
    lengths,
    state,
    gain_first,
    first_gate,
    first_up,
    first_down,
    gain_mix,
    query_weight,
    key_weight,
    value_weight,
    gating_weight,
    write_weight,
    forget_weight,
    forget_rate,
    out_weight,
    gain_second,
    second_gate,
    second_up,
    second_down,
):
    after_first = feed_forward(tokens, gain_first, first_gate, first_up, first_down)
    seq_count = lengths.shape[0]
    own_count = seq_count * BLK
    whole_rows = lax.all_gather(after_first, ("kv", "tp"), axis=1, tiled=True)
    scaled_all = (whole_rows.astype(jnp.float32) * gain_mix).astype(jnp.bfloat16)
    stacked = jnp.stack(
        [
            jnp.dot(scaled_all, matrix, preferred_element_type=jnp.float32)
            for matrix in (query_weight, key_weight, value_weight, gating_weight)
        ]
    )
    owned = lax.all_to_all(
        stacked.astype(jnp.bfloat16), ("kv", "tp"), split_axis=1, concat_axis=2, tiled=True
    ).astype(stacked.dtype)
    row_start = lax.axis_index(("kv", "tp")) * own_count
    own_values = lax.dynamic_slice_in_dim(whole_rows, row_start, own_count, 0).astype(jnp.float32)
    own_scaled = lax.dynamic_slice_in_dim(scaled_all, row_start, own_count, 0)
    mix_scale = lax.rsqrt(jnp.mean(own_values * own_values, axis=1, keepdims=True) + EPSILON)
    query = (owned[0] * mix_scale).reshape(seq_count, BLK, HEADS, HEAD)
    key_in = (owned[1] * mix_scale).reshape(seq_count, BLK, HEADS, HEAD)
    value = (owned[2] * mix_scale).reshape(seq_count, BLK, HEADS, HEAD)
    gating = (owned[3] * mix_scale).reshape(seq_count, BLK, HEADS, HEAD)
    write_pre = (
        jnp.dot(own_scaled, write_weight, preferred_element_type=jnp.float32) * mix_scale
    ).reshape(seq_count, BLK, HEADS)
    forget_pre = (
        jnp.dot(own_scaled, forget_weight, preferred_element_type=jnp.float32) * mix_scale
    ).reshape(seq_count, BLK, HEADS)
    positions = jnp.arange(BLK, dtype=jnp.int32)
    live = (positions[None, :] < lengths[:, None]).astype(jnp.float32)
    mixed_heads, new_state = delta_block(
        query, key_in, value, gating, write_pre, forget_pre, forget_rate, live, state
    )
    half_cols = mixed_heads.shape[1] // 2
    portion = lax.all_gather(mixed_heads, ("kv", "tp"), axis=0, tiled=True)
    first_half = jnp.dot(
        portion[:, :half_cols], out_weight[:half_cols], preferred_element_type=jnp.float32
    ).astype(jnp.bfloat16)
    second_half = jnp.dot(
        portion[:, half_cols:], out_weight[half_cols:], preferred_element_type=jnp.float32
    ).astype(jnp.bfloat16)
    first_half, second_half = lax.optimization_barrier((first_half, second_half))
    mixed_sum = first_half.astype(jnp.float32) + second_half.astype(jnp.float32)
    after_mix = (after_first.astype(jnp.float32) + mixed_sum).astype(jnp.bfloat16)
    mixed_out = feed_forward(after_mix, gain_second, second_gate, second_up, second_down)
    return (mixed_out, new_state)


def solution(mesh):
    in_specs = (
        P("dp", ("kv", "tp")),
        P(("dp", "kv", "tp")),
        P(("dp", "kv", "tp"), None, None, None),
        P(),
        P(None, "kv"),
        P(None, "kv"),
        P("kv", None),
        P(),
        P(None, ("kv", "tp")),
        P(None, ("kv", "tp")),
        P(None, ("kv", "tp")),
        P(None, ("kv", "tp")),
        P(),
        P(),
        P(),
        P(None, ("kv", "tp")),
        P(),
        P(None, "kv"),
        P(None, "kv"),
        P("kv", None),
    )
    out_specs = (P("dp", ("kv", "tp")), P(("dp", "kv", "tp"), None, None, None))
    return jax.shard_map(
        per_device, mesh=mesh, in_specs=in_specs, out_specs=out_specs, check_vma=False
    )
```

profile of v0, /device:TPU:0, one launch (start us, length us, event | category | flops | bytes accessed | tf_op | source)
XLA Modules:
  0.0 174.8 jit_solution(16179178874863830319)
XLA Ops:
  7.2 0.0 copy-start
  7.2 0.0 copy-start.4
  7.2 0.0 reduce-scatter.3.cloned.1.call-start
  7.2 4.8 %all_to_all.73 = bf16[2,32,256]{2,1,0:T(8,128)(2,1)S(1)} all-to-all(bf16[2,32,256]{2,1,0:T(8,128)(2,1)} %bitcast.150), channel_id=1, replica_groups=mesh['dp'=4,'kv'=4,'tp'=2] {'tp'}, dimensions={0} | all-to-all | bytes 65536 | tf_op jit(solution)/shard_map/all_to_all | solution.py:30
  12.0 15.1 %all_gather.12 = bf16[32,2048]{1,0:T(8,128)(2,1)S(1)} all-gather(bf16[32,512]{1,0:T(8,128)(2,1)S(1)} %bitcast.146), channel_id=1, replica_groups=mesh['dp'=4,'kv'=4,'tp'=2] {'kv'}, dimensions={1}, use_global_device_ids=true | all-gather | bytes 163840 | tf_op jit(solution)/shard_map/all_gather | solution.py:32
  27.1 0.1 fusion.25
  27.2 3.7 %convolution_multiply_fusion.3 = f32[32,1408]{1,0:T(8,128)S(1)} fusion(bf16[2048,1408]{1,0:T(8,128)(2,1)} %param.24, bf16[32,2048]{1,0:T(8,128)(2,1)S(1)} %all_gather.12, f32[2048]{0:T(1024)} %param.23, f32[32]{0:T(128)S(1)} %add_rsqrt_fusion.5), kind=kOutput, calls=%fused_computation.5 | convolution fusion | flops 184791040 | bytes 6086784 | tf_op jit(solution)/shard_map/dot_general | solution.py:16
  30.9 0.0 copy-start.8
  30.9 0.0 copy-start.3
  30.9 0.0 copy-start.6
  30.9 0.0 copy-start.2
  31.0 7.1 %fusion.21 = f32[32,2048]{1,0:T(8,128)} fusion(bf16[1408,2048]{1,0:T(8,128)(2,1)} %param.26, bf16[2048,1408]{1,0:T(8,128)(2,1)} %param.25, f32[32,1408]{1,0:T(8,128)S(1)} %convolution_multiply_fusion.3, bf16[32,2048]{1,0:T(8,128)(2,1)S(1)} %all_gather.12, f32[2048]{0:T(1024)S(1)} %copy-done.4, f32[32]{0:T(128)S(1)} %add_rsqrt_fusion.5), kind=kOutput, calls=%fused_computation.41 | convolution fusion | flops 369610752 | bytes 12116096 | tf_op jit(solution)/shard_map/dot_general | solution.py:25
  38.1 0.0 reduce-scatter.3.cloned.1.call-update
  38.9 20.5 %reduce-scatter.3.cloned.1.call-done = f32[32,512]{1,0:T(8,128)} async-done(((f32[32,2048]{1,0:T(8,128)}), f32[32,512]{1,0:T(8,128)}) %reduce-scatter.3.cloned.1.call-update) | async-done | bytes 65552 | tf_op jit(solution)/shard_map/reduce_scatter | solution.py:35
  59.4 0.8 copy.159
  60.2 3.8 %all_to_all.74 = f32[32,2,256]{2,0,1:T(8,128)S(1)} all-to-all(f32[32,2,256]{2,0,1:T(8,128)S(1)} %bitcast.144), channel_id=1, replica_groups=mesh['dp'=4,'kv'=4,'tp'=2] {'tp'}, dimensions={1} | all-to-all | bytes 131072 | tf_op jit(solution)/shard_map/all_to_all | solution.py:36
  64.0 14.3 %all_gather.13 = bf16[64,2048]{1,0:T(8,128)(2,1)S(1)} all-gather(bf16[64,256]{1,0:T(8,128)(2,1)S(1)} %fusion.51), channel_id=1, replica_groups=mesh['dp'=4,'kv'=4,'tp'=2] {'kv','tp'}, dimensions={1}, use_global_device_ids=true | all-gather | bytes 294912 | tf_op jit(solution)/shard_map/all_gather | solution.py:117
  78.4 0.1 multiply_reduce_fusion.1
  78.6 0.3 fusion.12
  78.9 0.3 fusion.11
  79.2 1.5 fusion.10
  80.7 1.5 fusion.9
  82.3 0.8 copy.99
  83.0 3.4 %all-to-all-start.2 = ((bf16[4,64,256]{2,0,1:T(4,128)(2,1)}), bf16[4,64,256]{2,0,1:T(4,128)(2,1)S(1)}, u32[]{:S(2)}, u32[]{:S(2)}) async-start(bf16[4,64,256]{2,0,1:T(4,128)(2,1)} %copy.99), calls=%async_computation.3 | async-start | bytes 262144 | tf_op jit(solution)/shard_map/all_to_all | solution.py:125
  86.4 0.0 reduce-scatter.5.cloned.1.call-start
  86.5 0.1 fusion.75
  86.7 0.1 copy.105
  86.7 0.9 fusion.80
  87.7 0.1 copy.104
  87.8 5.3 %all-to-all-done.2 = bf16[4,64,256]{2,0,1:T(4,128)(2,1)S(1)} async-done(((bf16[4,64,256]{2,0,1:T(4,128)(2,1)}), bf16[4,64,256]{2,0,1:T(4,128)(2,1)S(1)}, u32[]{:S(2)}, u32[]{:S(2)}) %all-to-all-start.2) | async-done | bytes 131104 | tf_op jit(solution)/shard_map/all_to_all | solution.py:125
  93.1 0.1 copy.157
  93.3 0.2 fusion.58
  93.5 0.1 copy.108
  93.5 0.1 copy.102
  93.6 0.2 fusion.67
  93.8 0.3 fusion.8
  94.1 0.3 fusion.88
  94.3 0.2 fusion.62
  94.6 0.3 convolution_add_fusion.1
  94.8 0.3 convolution_multiply_fusion.4
  95.1 0.1 broadcast_multiply_fusion.1
  95.2 0.3 fusion.89
  95.5 0.2 convolution_bitcast_fusion.2
  95.7 0.2 fusion.55
  96.0 1.0 convolution_bitcast_fusion.3
  96.9 1.0 fusion.7
  97.9 0.3 multiply_reduce_fusion
  98.3 0.1 copy.115
  98.3 0.1 copy.116
  98.4 0.1 fusion.70
  98.5 14.2 %all_gather.14 = bf16[64,2048]{1,0:T(8,128)(2,1)S(1)} all-gather(bf16[8,2048]{1,0:T(8,128)(2,1)S(1)} %fusion.70), channel_id=1, replica_groups=mesh['dp'=4,'kv'=4,'tp'=2] {'kv','tp'}, dimensions={0}, use_global_device_ids=true | all-gather | bytes 294912 | tf_op jit(solution)/shard_map/all_gather | solution.py:148
  112.8 1.2 convolution_convert_fusion
  114.0 1.2 convolution_convert_fusion.1
  115.3 3.7 %all_to_all.75 = bf16[2,32,256]{2,1,0:T(8,128)(2,1)S(1)} all-to-all(bf16[2,32,256]{2,1,0:T(8,128)(2,1)S(1)} %bitcast.143), channel_id=1, replica_groups=mesh['dp'=4,'kv'=4,'tp'=2] {'tp'}, dimensions={0} | all-to-all | bytes 65536 | tf_op jit(solution)/shard_map/all_to_all | solution.py:30
  119.0 13.6 %all_gather.15 = bf16[32,2048]{1,0:T(8,128)(2,1)S(1)} all-gather(bf16[32,512]{1,0:T(8,128)(2,1)S(1)} %bitcast.147), channel_id=1, replica_groups=mesh['dp'=4,'kv'=4,'tp'=2] {'kv'}, dimensions={1}, use_global_device_ids=true | all-gather | bytes 163840 | tf_op jit(solution)/shard_map/all_gather | solution.py:32
  132.6 0.1 fusion.27
  132.7 3.6 %convolution_multiply_fusion.1 = f32[32,1408]{1,0:T(8,128)S(1)} fusion(bf16[2048,1408]{1,0:T(8,128)(2,1)} %param.37, bf16[32,2048]{1,0:T(8,128)(2,1)S(1)} %all_gather.15, f32[2048]{0:T(1024)S(1)} %copy-done.5, f32[32]{0:T(128)S(1)} %add_rsqrt_fusion.3), kind=kOutput, calls=%fused_computation.2 | convolution fusion | flops 184791040 | bytes 6086784 | tf_op jit(solution)/shard_map/dot_general | solution.py:16
  136.4 7.0 %fusion.20 = f32[32,2048]{1,0:T(8,128)} fusion(bf16[1408,2048]{1,0:T(8,128)(2,1)} %param.39, bf16[2048,1408]{1,0:T(8,128)(2,1)} %param.38, f32[32,1408]{1,0:T(8,128)S(1)} %convolution_multiply_fusion.1, bf16[32,2048]{1,0:T(8,128)(2,1)S(1)} %all_gather.15, f32[2048]{0:T(1024)S(1)} %copy-done.5, f32[32]{0:T(128)S(1)} %add_rsqrt_fusion.3), kind=kOutput, calls=%fused_computation.40 | convolution fusion | flops 369610752 | bytes 12116096 | tf_op jit(solution)/shard_map/dot_general | solution.py:25
  143.4 0.0 reduce-scatter.5.cloned.1.call-update
  143.5 2.8 %fusion.4 = f32[1,16,128,128]{3,2,1,0:T(8,128)} fusion(f32[8,16,128]{2,0,1:T(8,128)S(1)} %fusion.7, f32[1,16,128,128]{3,2,1,0:T(8,128)S(1)} %copy-done.1, f32[16]{0:T(128)S(1)} %fusion.86, f32[8,16,128]{2,1,0:T(8,128)S(1)} %get-tuple-element.20), kind=kOutput, calls=%fused_computation.9 | convolution fusion | flops 25690112 | bytes 2228288 | tf_op jit(solution)/shard_map/sthk,sthv->shkv/dot_general | solution.py:83
  146.3 16.4 %reduce-scatter.5.cloned.1.call-done = f32[32,512]{1,0:T(8,128)} async-done(((f32[32,2048]{1,0:T(8,128)}), f32[32,512]{1,0:T(8,128)}) %reduce-scatter.5.cloned.1.call-update) | async-done | bytes 65552 | tf_op jit(solution)/shard_map/reduce_scatter | solution.py:35
  162.7 0.8 copy.158
  163.6 3.8 %all_to_all.76 = f32[32,2,256]{2,0,1:T(8,128)S(1)} all-to-all(f32[32,2,256]{2,0,1:T(8,128)S(1)} %bitcast.145), channel_id=1, replica_groups=mesh['dp'=4,'kv'=4,'tp'=2] {'tp'}, dimensions={1} | all-to-all | bytes 131072 | tf_op jit(solution)/shard_map/all_to_all | solution.py:36
  167.4 0.6 fusion.50
  (39 shorter events, 0.3 us)
Async XLA Ops:
  7.2 71.4 %copy-start = (bf16[2048,256]{1,0:T(8,128)(2,1)S(1)}, bf16[2048,256]{1,0:T(8,128)(2,1)}, u32[]{:S(2)}) copy-start(bf16[2048,256]{1,0:T(8,128)(2,1)} %param.31) | copy-start | bytes 3145732
  7.2 23.7 %copy-start.4 = (f32[2048]{0:T(1024)S(1)}, f32[2048]{0:T(1024)}, u32[]{:S(2)}) copy-start(f32[2048]{0:T(1024)} %param.23) | copy-start | bytes 24580
  7.2 52.2 %reduce-scatter.3.cloned.1.call-start = ((), (), s32[]{:S(2)}) async-start(), calls=%async_computation.7 | async-start | bytes 327680 | tf_op jit(solution)/shard_map/reduce_scatter | solution.py:35
  30.9 7.9 %copy-start.8 = (f32[16]{0:T(128)S(1)}, f32[16]{0:T(128)}, u32[]{:S(2)}) copy-start(f32[16]{0:T(128)} %param.34) | copy-start | bytes 196
  30.9 33.1 %copy-start.3 = (bf16[64,256]{1,0:T(8,128)(2,1)S(1)}, bf16[64,256]{1,0:T(8,128)(2,1)}, u32[]{:S(2)}) copy-start(bf16[64,256]{1,0:T(8,128)(2,1)} %param.20) | copy-start | bytes 98308
  30.9 47.6 %copy-start.6 = (f32[2048]{0:T(1024)S(1)}, f32[2048]{0:T(1024)}, u32[]{:S(2)}) copy-start(f32[2048]{0:T(1024)} %param.27) | copy-start | bytes 24580
  30.9 47.9 %copy-start.2 = (bf16[2048,256]{1,0:T(8,128)(2,1)S(1)}, bf16[2048,256]{1,0:T(8,128)(2,1)}, u32[]{:S(2)}) copy-start(bf16[2048,256]{1,0:T(8,128)(2,1)} %param.30) | copy-start | bytes 3145732
  38.1 48.4 %copy-start.7 = (bf16[2048,16]{0,1:T(8,128)(2,1)S(1)}, bf16[2048,16]{0,1:T(8,128)(2,1)}, u32[]{:S(2)}) copy-start(bf16[2048,16]{0,1:T(8,128)(2,1)} %param.33) | copy-start | bytes 196612
  64.0 31.9 %copy-start.1 = (f32[1,16,128,128]{3,2,1,0:T(8,128)S(1)}, f32[1,16,128,128]{3,2,1,0:T(8,128)}, u32[]{:S(2)}) copy-start(f32[1,16,128,128]{3,2,1,0:T(8,128)} %param.22) | copy-start | bytes 3145732
  80.7 52.0 %copy-start.5 = (f32[2048]{0:T(1024)S(1)}, f32[2048]{0:T(1024)}, u32[]{:S(2)}) copy-start(f32[2048]{0:T(1024)} %param.36) | copy-start | bytes 24580
  83.0 10.1 %all-to-all-start.2 = ((bf16[4,64,256]{2,0,1:T(4,128)(2,1)}), bf16[4,64,256]{2,0,1:T(4,128)(2,1)S(1)}, u32[]{:S(2)}, u32[]{:S(2)}) async-start(bf16[4,64,256]{2,0,1:T(4,128)(2,1)} %copy.99), calls=%async_computation.3 | async-start | bytes 262144 | tf_op jit(solution)/shard_map/all_to_all | solution.py:125
  86.4 76.3 %reduce-scatter.5.cloned.1.call-start = ((), (), s32[]{:S(2)}) async-start(), calls=%async_computation.8 | async-start | bytes 327680 | tf_op jit(solution)/shard_map/reduce_scatter | solution.py:35
Sparse Core Ops, SparseCore 0:
  38.2 21.0 reduce-scatter.2
  143.6 19.1 reduce-scatter.4
where the time goes:
time: 176 us; the launch traced here: 175 us
  blocking collectives  73.2 us (42%)
  waiting for transfers between devices  42.3 us (24%)
  matrix products  35.8 us (20%)
  between operations  15.2 us (9%)
  starting transfers between devices  3.45 us (2%)
  local copies, waits for them, and re-layouts  3.13 us (2%)
  other arithmetic  1.76 us (1%)
    reduce_scatter x2, waiting for transfers between devices, feed_forward(): lax.psum_scatter(ffn_term, 'kv', scatter_dimension=1, tiled=True)  36.9 us
    all_gather x2, blocking collectives, feed_forward(): lax.all_gather(paired, 'kv', axis=1, tiled=True)  28.6 us
    all_gather x1, blocking collectives, per_device(): whole_rows = lax.all_gather(after_first, ('kv', 'tp'), axis=1, tiled=True)  14.3 us
    all_gather x1, blocking collectives, per_device(): portion = lax.all_gather(mixed_heads, ('kv', 'tp'), axis=0, tiled=True)  14.2 us
    dot_general x2, matrix products, finish_units(): return jnp.dot(hidden, down_rows, preferred_element_type=jnp.float32)  14.2 us
    all_to_all x2, blocking collectives, feed_forward(): lax.all_to_all(hidden_in, 'tp', split_axis=0, concat_axis=1, tiled=True)  8.52 us
    all_to_all x2, blocking collectives, feed_forward(): lax.all_to_all(partial_value, 'tp', split_axis=1, concat_axis=0, tiled=True)  7.56 us
    dot_general x2, matrix products, fold_step(): gate_acc = jnp.dot(scaled, gate_cols, preferred_element_type=jnp.float32)  7.31 us
  transfers between devices with their start and end apart: 3, of which 3 were waited for; matrix products, arithmetic and copies ran while one was open for 2% of the time, Pallas kernels for 0%

commit v1 on v0

--- a/solution.py
+++ b/solution.py
@@ -1,3 +1,4 @@
+import functools
 import math
 import jax
 import jax.numpy as jnp
@@ -8,6 +9,34 @@
 HEAD = 128
 BLK = 8
 EPSILON = 1e-06
+
+
+def obtain_the_plane(slab_in, across):
+    formed, prior, carry_in = (
+        jax.lax.axis_size(across),
+        jax.lax.axis_index(across),
+        slab_in.shape[1],
+    )
+    tray = [(j, (j + 1) % formed) for j in range(formed)]
+    trail = [(j, (j - 1) % formed) for j in range(formed)]
+    carry = jnp.zeros((*slab_in.shape[:1], formed * carry_in, *slab_in.shape[2:]), slab_in.dtype)
+    carry = lax.dynamic_update_slice_in_dim(carry, slab_in, prior * carry_in, axis=1)
+    kept_arr = row_out = slab_in
+    mid_arr = formed // 2
+    for idx in tuple(range(1, mid_arr + 1)):
+        kept_arr = jax.lax.ppermute(kept_arr, across, tray)
+        carry = lax.dynamic_update_slice_in_dim(
+            carry, kept_arr, (prior - idx) % formed * carry_in, axis=1
+        )
+        if idx < formed - mid_arr:
+            row_out = jax.lax.ppermute(row_out, across, trail)
+            carry = lax.dynamic_update_slice_in_dim(
+                carry, row_out, (prior + idx) % formed * carry_in, axis=1
+            )
+    return carry
+
+
+_link_links = functools.partial(obtain_the_plane, across=("kv", "tp"))
 
 
 def fold_step(gain, gate_cols, up_cols, portion):
@@ -114,7 +143,7 @@
     after_first = feed_forward(tokens, gain_first, first_gate, first_up, first_down)
     seq_count = lengths.shape[0]
     own_count = seq_count * BLK
-    whole_rows = lax.all_gather(after_first, ("kv", "tp"), axis=1, tiled=True)
+    whole_rows = _link_links(after_first)
     scaled_all = (whole_rows.astype(jnp.float32) * gain_mix).astype(jnp.bfloat16)
     stacked = jnp.stack(
         [

time: 176 us -> 183 us (1.040)
  blocking collectives: 73.2 us -> 58.9 us
  starting transfers between devices: 3.45 us -> 14.2 us
  waiting for transfers between devices: 42.3 us -> 52.9 us
    all_gather x1 -> x0, blocking collectives: 14.3 us -> none  [per_device(): whole_rows = lax.all_gather(after_first, ('kv', 'tp'), axis=1, tiled=True)]
    ppermute x0 -> x7, starting transfers between devices: none -> 10.8 us  [the longest x3 10.6 us: obtain_the_plane(): row_out = jax.lax.ppermute(row_out, across, trail)]
    ppermute x0 -> x7, waiting for transfers between devices: none -> 9.8 us  [the longest x4 9.71 us: obtain_the_plane(): kept_arr = jax.lax.ppermute(kept_arr, across, tray)]
  transfers between devices with their start and end apart: 3 -> 10, of which waited for: 3 -> 8; matrix products, arithmetic and copies ran while one was open for 2% -> 2% of each run, Pallas kernels for 0% -> 0%
where the time goes in v1:
time: 183 us; the launch traced here: 182 us
  blocking collectives  58.9 us (32%)
  waiting for transfers between devices  52.9 us (29%)
  matrix products  36.1 us (20%)
  between operations  15.2 us (8%)
  starting transfers between devices  14.2 us (8%)
  local copies, waits for them, and re-layouts  3.13 us (2%)
    reduce_scatter x2, waiting for transfers between devices, feed_forward(): lax.psum_scatter(ffn_term, 'kv', scatter_dimension=1, tiled=True)  36.9 us
    all_gather x2, blocking collectives, feed_forward(): lax.all_gather(paired, 'kv', axis=1, tiled=True)  28.6 us
    all_gather x1, blocking collectives, per_device(): portion = lax.all_gather(mixed_heads, ('kv', 'tp'), axis=0, tiled=True)  14.2 us
    dot_general x2, matrix products, finish_units(): return jnp.dot(hidden, down_rows, preferred_element_type=jnp.float32)  14.1 us
    ppermute x3, starting transfers between devices, obtain_the_plane(): row_out = jax.lax.ppermute(row_out, across, trail)  10.6 us
    ppermute x4, waiting for transfers between devices, obtain_the_plane(): kept_arr = jax.lax.ppermute(kept_arr, across, tray)  9.71 us
    all_to_all x2, blocking collectives, feed_forward(): lax.all_to_all(hidden_in, 'tp', split_axis=0, concat_axis=1, tiled=True)  8.52 us
    all_to_all x2, blocking collectives, feed_forward(): lax.all_to_all(partial_value, 'tp', split_axis=1, concat_axis=0, tiled=True)  7.56 us
  transfers between devices with their start and end apart: 10, of which 8 were waited for; matrix products, arithmetic and copies ran while one was open for 2% of the time, Pallas kernels for 0%

profile of v1, /device:TPU:0, one launch (start us, length us, event | category | flops | bytes accessed | tf_op | source)
XLA Modules:
  0.0 182.2 jit_solution(6646317066628369878)
XLA Ops:
  7.2 0.0 reduce-scatter.3.cloned.1.call-start
  7.2 4.8 %all_to_all.73 = bf16[2,32,256]{2,1,0:T(8,128)(2,1)S(1)} all-to-all(bf16[2,32,256]{2,1,0:T(8,128)(2,1)} %bitcast.146), channel_id=1, replica_groups=mesh['dp'=4,'kv'=4,'tp'=2] {'tp'}, dimensions={0} | all-to-all | bytes 65536 | tf_op jit(solution)/shard_map/all_to_all | solution.py:59
  12.0 15.1 %all_gather.9 = bf16[32,2048]{1,0:T(8,128)(2,1)S(1)} all-gather(bf16[32,512]{1,0:T(8,128)(2,1)S(1)} %bitcast.147), channel_id=1, replica_groups=mesh['dp'=4,'kv'=4,'tp'=2] {'kv'}, dimensions={1}, use_global_device_ids=true | all-gather | bytes 163840 | tf_op jit(solution)/shard_map/all_gather | solution.py:61
  27.1 0.1 fusion.25
  27.2 3.7 %convolution_multiply_fusion.3 = f32[32,1408]{1,0:T(8,128)S(1)} fusion(bf16[2048,1408]{1,0:T(8,128)(2,1)} %param.24, bf16[32,2048]{1,0:T(8,128)(2,1)S(1)} %all_gather.9, f32[2048]{0:T(1024)} %param.23, f32[32]{0:T(128)S(1)} %add_rsqrt_fusion.5), kind=kOutput, calls=%fused_computation.5 | convolution fusion | flops 184791040 | bytes 6086784 | tf_op jit(solution)/shard_map/dot_general | solution.py:45
  30.9 7.1 %fusion.21 = f32[32,2048]{1,0:T(8,128)} fusion(bf16[1408,2048]{1,0:T(8,128)(2,1)} %param.26, bf16[2048,1408]{1,0:T(8,128)(2,1)} %param.25, f32[32,1408]{1,0:T(8,128)S(1)} %convolution_multiply_fusion.3, bf16[32,2048]{1,0:T(8,128)(2,1)S(1)} %all_gather.9, f32[2048]{0:T(1024)S(1)} %copy-done.3, f32[32]{0:T(128)S(1)} %add_rsqrt_fusion.5), kind=kOutput, calls=%fused_computation.41 | convolution fusion | flops 369610752 | bytes 12116096 | tf_op jit(solution)/shard_map/dot_general | solution.py:54
  38.8 20.5 %reduce-scatter.3.cloned.1.call-done = f32[32,512]{1,0:T(8,128)} async-done(((f32[32,2048]{1,0:T(8,128)}), f32[32,512]{1,0:T(8,128)}) %reduce-scatter.3.cloned.1.call-update) | async-done | bytes 65552 | tf_op jit(solution)/shard_map/reduce_scatter | solution.py:64
  59.3 0.8 copy.159
  60.1 3.8 %all_to_all.74 = f32[32,2,256]{2,0,1:T(8,128)S(1)} all-to-all(f32[32,2,256]{2,0,1:T(8,128)S(1)} %bitcast.144), channel_id=1, replica_groups=mesh['dp'=4,'kv'=4,'tp'=2] {'tp'}, dimensions={1} | all-to-all | bytes 131072 | tf_op jit(solution)/shard_map/all_to_all | solution.py:65
  64.0 0.2 collective-permute-start
  64.2 3.4 %collective-permute-start.1 = (bf16[64,256]{1,0:T(8,128)(2,1)S(1)}, bf16[64,256]{1,0:T(8,128)(2,1)S(1)}, u32[]{:S(2)}, u32[]{:S(2)}) collective-permute-start(bf16[64,256]{1,0:T(8,128)(2,1)S(1)} %get-tuple-element.23), channel_id=1, source_target_pairs={{0,7},{1,0},{2,1},{3,2},{4,3},{5,4},{6,5},{7,6},{8,15},{9,8},{10,9... | collective-permute-start | bytes 98312 | tf_op jit(solution)/shard_map/ppermute | solution.py:32
  67.6 1.6 collective-permute-done
  69.2 3.5 %collective-permute-start.3 = (bf16[64,256]{1,0:T(8,128)(2,1)S(1)}, bf16[64,256]{1,0:T(8,128)(2,1)S(1)}, u32[]{:S(2)}, u32[]{:S(2)}) collective-permute-start(bf16[64,256]{1,0:T(8,128)(2,1)S(1)} %collective-permute-done.1), channel_id=1, source_target_pairs={{0,7},{1,0},{2,1},{3,2},{4,3},{5,4},{6,5},{7,6},{8,15},{9,8},{10,9... | collective-permute-start | bytes 98312 | tf_op jit(solution)/shard_map/ppermute | solution.py:32
  72.7 1.6 collective-permute-done.2
  74.3 3.6 %collective-permute-start.5 = (bf16[64,256]{1,0:T(8,128)(2,1)S(1)}, bf16[64,256]{1,0:T(8,128)(2,1)S(1)}, u32[]{:S(2)}, u32[]{:S(2)}) collective-permute-start(bf16[64,256]{1,0:T(8,128)(2,1)S(1)} %collective-permute-done.3), channel_id=1, source_target_pairs={{0,7},{1,0},{2,1},{3,2},{4,3},{5,4},{6,5},{7,6},{8,15},{9,8},{10,9... | collective-permute-start | bytes 98312 | tf_op jit(solution)/shard_map/ppermute | solution.py:32
  78.0 1.5 collective-permute-done.4
  79.5 0.1 collective-permute-done.5
  79.6 5.0 %collective-permute-done.6 = bf16[64,256]{1,0:T(8,128)(2,1)S(1)} collective-permute-done((bf16[64,256]{1,0:T(8,128)(2,1)S(1)}, bf16[64,256]{1,0:T(8,128)(2,1)S(1)}, u32[]{:S(2)}, u32[]{:S(2)}) %collective-permute-start.6) | collective-permute-done | bytes 32800 | tf_op jit(solution)/shard_map/ppermute | solution.py:27
  84.6 0.1 multiply_reduce_fusion.1
  84.8 0.3 fusion.12
  85.1 1.5 fusion.11
  86.6 1.5 fusion.10
  88.2 1.5 fusion.9
  89.7 0.8 copy.99
  90.5 3.4 %all-to-all-start.2 = ((bf16[4,64,256]{2,0,1:T(4,128)(2,1)}), bf16[4,64,256]{2,0,1:T(4,128)(2,1)S(1)}, u32[]{:S(2)}, u32[]{:S(2)}) async-start(bf16[4,64,256]{2,0,1:T(4,128)(2,1)} %copy.99), calls=%async_computation.3 | async-start | bytes 262144 | tf_op jit(solution)/shard_map/all_to_all | solution.py:154
  93.9 0.0 reduce-scatter.5.cloned.1.call-start
  93.9 0.1 fusion.75
  94.1 0.1 copy.105
  94.2 0.1 fusion.80
  94.3 0.1 copy.104
  94.4 6.2 %all-to-all-done.2 = bf16[4,64,256]{2,0,1:T(4,128)(2,1)S(1)} async-done(((bf16[4,64,256]{2,0,1:T(4,128)(2,1)}), bf16[4,64,256]{2,0,1:T(4,128)(2,1)S(1)}, u32[]{:S(2)}, u32[]{:S(2)}) %all-to-all-start.2) | async-done | bytes 131104 | tf_op jit(solution)/shard_map/all_to_all | solution.py:154
  100.6 0.1 copy.157
  100.7 0.2 fusion.58
  100.9 0.1 copy.108
  101.0 0.1 copy.102
  101.1 0.2 fusion.67
  101.3 0.3 fusion.8
  101.5 0.2 fusion.88
  101.8 0.2 fusion.62
  102.0 0.3 convolution_add_fusion.1
  102.3 0.3 convolution_multiply_fusion.4
  102.6 0.1 broadcast_multiply_fusion.1
  102.7 0.2 fusion.89
  102.9 0.2 convolution_bitcast_fusion.2
  103.2 0.2 fusion.55
  103.4 1.0 convolution_bitcast_fusion.3
  104.4 1.0 fusion.7
  105.4 0.3 multiply_reduce_fusion
  105.7 0.1 copy.115
  105.8 0.1 copy.116
  105.9 0.1 fusion.70
  106.0 14.2 %all_gather.10 = bf16[64,2048]{1,0:T(8,128)(2,1)S(1)} all-gather(bf16[8,2048]{1,0:T(8,128)(2,1)S(1)} %fusion.70), channel_id=1, replica_groups=mesh['dp'=4,'kv'=4,'tp'=2] {'kv','tp'}, dimensions={0}, use_global_device_ids=true | all-gather | bytes 294912 | tf_op jit(solution)/shard_map/all_gather | solution.py:177
  120.2 1.2 convolution_convert_fusion
  121.5 1.2 convolution_convert_fusion.1
  122.7 3.7 %all_to_all.75 = bf16[2,32,256]{2,1,0:T(8,128)(2,1)S(1)} all-to-all(bf16[2,32,256]{2,1,0:T(8,128)(2,1)S(1)} %bitcast.143), channel_id=1, replica_groups=mesh['dp'=4,'kv'=4,'tp'=2] {'tp'}, dimensions={0} | all-to-all | bytes 65536 | tf_op jit(solution)/shard_map/all_to_all | solution.py:59
  126.5 13.6 %all_gather.11 = bf16[32,2048]{1,0:T(8,128)(2,1)S(1)} all-gather(bf16[32,512]{1,0:T(8,128)(2,1)S(1)} %bitcast.148), channel_id=1, replica_groups=mesh['dp'=4,'kv'=4,'tp'=2] {'kv'}, dimensions={1}, use_global_device_ids=true | all-gather | bytes 163840 | tf_op jit(solution)/shard_map/all_gather | solution.py:61
  140.0 0.1 fusion.27
  140.2 3.6 %convolution_multiply_fusion.1 = f32[32,1408]{1,0:T(8,128)S(1)} fusion(bf16[2048,1408]{1,0:T(8,128)(2,1)} %param.37, bf16[32,2048]{1,0:T(8,128)(2,1)S(1)} %all_gather.11, f32[2048]{0:T(1024)S(1)} %copy-done.4, f32[32]{0:T(128)S(1)} %add_rsqrt_fusion.3), kind=kOutput, calls=%fused_computation.2 | convolution fusion | flops 184791040 | bytes 6086784 | tf_op jit(solution)/shard_map/dot_general | solution.py:45
  143.8 7.0 %fusion.20 = f32[32,2048]{1,0:T(8,128)} fusion(bf16[1408,2048]{1,0:T(8,128)(2,1)} %param.39, bf16[2048,1408]{1,0:T(8,128)(2,1)} %param.38, f32[32,1408]{1,0:T(8,128)S(1)} %convolution_multiply_fusion.1, bf16[32,2048]{1,0:T(8,128)(2,1)S(1)} %all_gather.11, f32[2048]{0:T(1024)S(1)} %copy-done.4, f32[32]{0:T(128)S(1)} %add_rsqrt_fusion.3), kind=kOutput, calls=%fused_computation.40 | convolution fusion | flops 369610752 | bytes 12116096 | tf_op jit(solution)/shard_map/dot_general | solution.py:54
  150.9 2.8 %fusion.4 = f32[1,16,128,128]{3,2,1,0:T(8,128)} fusion(f32[8,16,128]{2,0,1:T(8,128)S(1)} %fusion.7, f32[1,16,128,128]{3,2,1,0:T(8,128)S(1)} %copy-done.1, f32[16]{0:T(128)S(1)} %fusion.86, f32[8,16,128]{2,1,0:T(8,128)S(1)} %get-tuple-element.20), kind=kOutput, calls=%fused_computation.9 | convolution fusion | flops 25690112 | bytes 2228288 | tf_op jit(solution)/shard_map/sthk,sthv->shkv/dot_general | solution.py:112
  153.8 16.4 %reduce-scatter.5.cloned.1.call-done = f32[32,512]{1,0:T(8,128)} async-done(((f32[32,2048]{1,0:T(8,128)}), f32[32,512]{1,0:T(8,128)}) %reduce-scatter.5.cloned.1.call-update) | async-done | bytes 65552 | tf_op jit(solution)/shard_map/reduce_scatter | solution.py:64
  170.1 0.8 copy.158
  171.0 3.8 %all_to_all.76 = f32[32,2,256]{2,0,1:T(8,128)S(1)} all-to-all(f32[32,2,256]{2,0,1:T(8,128)S(1)} %bitcast.145), channel_id=1, replica_groups=mesh['dp'=4,'kv'=4,'tp'=2] {'tp'}, dimensions={1} | all-to-all | bytes 131072 | tf_op jit(solution)/shard_map/all_to_all | solution.py:65
  174.8 0.6 fusion.50
  (60 shorter events, 0.4 us)
Async XLA Ops:
  7.2 77.6 %copy-start = (bf16[2048,256]{1,0:T(8,128)(2,1)S(1)}, bf16[2048,256]{1,0:T(8,128)(2,1)}, u32[]{:S(2)}) copy-start(bf16[2048,256]{1,0:T(8,128)(2,1)} %param.31) | copy-start | bytes 3145732
  7.2 23.7 %copy-start.3 = (f32[2048]{0:T(1024)S(1)}, f32[2048]{0:T(1024)}, u32[]{:S(2)}) copy-start(f32[2048]{0:T(1024)} %param.23) | copy-start | bytes 24580
  7.2 52.1 %reduce-scatter.3.cloned.1.call-start = ((), (), s32[]{:S(2)}) async-start(), calls=%async_computation.7 | async-start | bytes 327680 | tf_op jit(solution)/shard_map/reduce_scatter | solution.py:64
  30.9 7.8 %copy-start.8 = (f32[16]{0:T(128)S(1)}, f32[16]{0:T(128)}, u32[]{:S(2)}) copy-start(f32[16]{0:T(128)} %param.34) | copy-start | bytes 196
  30.9 33.0 %copy-start.2 = (bf16[64,256]{1,0:T(8,128)(2,1)S(1)}, bf16[64,256]{1,0:T(8,128)(2,1)}, u32[]{:S(2)}) copy-start(bf16[64,256]{1,0:T(8,128)(2,1)} %param.20) | copy-start | bytes 98308
  30.9 53.8 %copy-start.5 = (f32[2048]{0:T(1024)S(1)}, f32[2048]{0:T(1024)}, u32[]{:S(2)}) copy-start(f32[2048]{0:T(1024)} %param.27) | copy-start | bytes 24580
  38.0 55.9 %copy-start.6 = (bf16[2048,16]{0,1:T(8,128)(2,1)S(1)}, bf16[2048,16]{0,1:T(8,128)(2,1)}, u32[]{:S(2)}) copy-start(bf16[2048,16]{0,1:T(8,128)(2,1)} %param.33) | copy-start | bytes 196612
  38.0 56.2 %copy-start.7 = (bf16[2048,16]{0,1:T(8,128)(2,1)S(1)}, bf16[2048,16]{0,1:T(8,128)(2,1)}, u32[]{:S(2)}) copy-start(bf16[2048,16]{0,1:T(8,128)(2,1)} %param.32) | copy-start | bytes 196612
  64.0 5.2 %collective-permute-start = (bf16[64,256]{1,0:T(8,128)(2,1)S(1)}, bf16[64,256]{1,0:T(8,128)(2,1)S(1)}, u32[]{:S(2)}, u32[]{:S(2)}) collective-permute-start(bf16[64,256]{1,0:T(8,128)(2,1)S(1)} %get-tuple-element.23), channel_id=1, source_target_pairs={{0,1},{1,2},{2,3},{3,4},{4,5},{5,6},{6,7},{7,0},{8,9},{9,10},{10,1... | collective-permute-start | bytes 98312 | tf_op jit(solution)/shard_map/ppermute | solution.py:27
  64.2 5.0 %collective-permute-start.1 = (bf16[64,256]{1,0:T(8,128)(2,1)S(1)}, bf16[64,256]{1,0:T(8,128)(2,1)S(1)}, u32[]{:S(2)}, u32[]{:S(2)}) collective-permute-start(bf16[64,256]{1,0:T(8,128)(2,1)S(1)} %get-tuple-element.23), channel_id=1, source_target_pairs={{0,7},{1,0},{2,1},{3,2},{4,3},{5,4},{6,5},{7,6},{8,15},{9,8},{10,9... | collective-permute-start | bytes 98312 | tf_op jit(solution)/shard_map/ppermute | solution.py:32
  69.2 5.2 %collective-permute-start.2 = (bf16[64,256]{1,0:T(8,128)(2,1)S(1)}, bf16[64,256]{1,0:T(8,128)(2,1)S(1)}, u32[]{:S(2)}, u32[]{:S(2)}) collective-permute-start(bf16[64,256]{1,0:T(8,128)(2,1)S(1)} %collective-permute-done), channel_id=1, source_target_pairs={{0,1},{1,2},{2,3},{3,4},{4,5},{5,6},{6,7},{7,0},{8,9},{9,10},{10,1... | collective-permute-start | bytes 98312 | tf_op jit(solution)/shard_map/ppermute | solution.py:27
  69.2 5.2 %collective-permute-start.3 = (bf16[64,256]{1,0:T(8,128)(2,1)S(1)}, bf16[64,256]{1,0:T(8,128)(2,1)S(1)}, u32[]{:S(2)}, u32[]{:S(2)}) collective-permute-start(bf16[64,256]{1,0:T(8,128)(2,1)S(1)} %collective-permute-done.1), channel_id=1, source_target_pairs={{0,7},{1,0},{2,1},{3,2},{4,3},{5,4},{6,5},{7,6},{8,15},{9,8},{10,9... | collective-permute-start | bytes 98312 | tf_op jit(solution)/shard_map/ppermute | solution.py:32
  74.3 5.1 %collective-permute-start.4 = (bf16[64,256]{1,0:T(8,128)(2,1)S(1)}, bf16[64,256]{1,0:T(8,128)(2,1)S(1)}, u32[]{:S(2)}, u32[]{:S(2)}) collective-permute-start(bf16[64,256]{1,0:T(8,128)(2,1)S(1)} %collective-permute-done.2), channel_id=1, source_target_pairs={{0,1},{1,2},{2,3},{3,4},{4,5},{5,6},{6,7},{7,0},{8,9},{9,10},{10,1... | collective-permute-start | bytes 98312 | tf_op jit(solution)/shard_map/ppermute | solution.py:27
  74.3 5.2 %collective-permute-start.5 = (bf16[64,256]{1,0:T(8,128)(2,1)S(1)}, bf16[64,256]{1,0:T(8,128)(2,1)S(1)}, u32[]{:S(2)}, u32[]{:S(2)}) collective-permute-start(bf16[64,256]{1,0:T(8,128)(2,1)S(1)} %collective-permute-done.3), channel_id=1, source_target_pairs={{0,7},{1,0},{2,1},{3,2},{4,3},{5,4},{6,5},{7,6},{8,15},{9,8},{10,9... | collective-permute-start | bytes 98312 | tf_op jit(solution)/shard_map/ppermute | solution.py:32
  78.0 25.4 %copy-start.1 = (f32[1,16,128,128]{3,2,1,0:T(8,128)S(1)}, f32[1,16,128,128]{3,2,1,0:T(8,128)}, u32[]{:S(2)}) copy-start(f32[1,16,128,128]{3,2,1,0:T(8,128)} %param.22) | copy-start | bytes 3145732
  79.5 5.1 %collective-permute-start.6 = (bf16[64,256]{1,0:T(8,128)(2,1)S(1)}, bf16[64,256]{1,0:T(8,128)(2,1)S(1)}, u32[]{:S(2)}, u32[]{:S(2)}) collective-permute-start(bf16[64,256]{1,0:T(8,128)(2,1)S(1)} %collective-permute-done.4), channel_id=1, source_target_pairs={{0,1},{1,2},{2,3},{3,4},{4,5},{5,6},{6,7},{7,0},{8,9},{9,10},{10,1... | collective-permute-start | bytes 98312 | tf_op jit(solution)/shard_map/ppermute | solution.py:27
  88.2 52.0 %copy-start.4 = (f32[2048]{0:T(1024)S(1)}, f32[2048]{0:T(1024)}, u32[]{:S(2)}) copy-start(f32[2048]{0:T(1024)} %param.36) | copy-start | bytes 24580
  90.5 10.1 %all-to-all-start.2 = ((bf16[4,64,256]{2,0,1:T(4,128)(2,1)}), bf16[4,64,256]{2,0,1:T(4,128)(2,1)S(1)}, u32[]{:S(2)}, u32[]{:S(2)}) async-start(bf16[4,64,256]{2,0,1:T(4,128)(2,1)} %copy.99), calls=%async_computation.3 | async-start | bytes 262144 | tf_op jit(solution)/shard_map/all_to_all | solution.py:154
  93.9 76.3 %reduce-scatter.5.cloned.1.call-start = ((), (), s32[]{:S(2)}) async-start(), calls=%async_computation.8 | async-start | bytes 327680 | tf_op jit(solution)/shard_map/reduce_scatter | solution.py:64
Sparse Core Ops, SparseCore 0:
  38.2 21.0 reduce-scatter.2
  151.0 19.0 reduce-scatter.4
